TPU v7x, 512 devices: a whole 4x8x8 slice. The times are simulated.
512 devices in a mesh: ep: 128 (over z, y, core), tp: 4 (over x).
Axes of the slice: x: 4, y: 8, z: 8, core: 2. Of those that a mesh axis runs over, the one named last changes fastest.
Arguments:
- tokens: bfloat16 [8192, 1024], P('ep', 'tp'), may hold values from -6 to 6
- conv_state: bfloat16 [8192, 3, 512], P('ep', None, 'tp'), may hold values from -6 to 6
- lru_state: float32 [8192, 512], P('ep', 'tp'), may hold values from -6 to 6
- mix_gain: bfloat16 [1024], replicated, may hold values from 0.099609375 to 1.8984375
- ffn_gain: bfloat16 [1024], replicated, may hold values from 0.099609375 to 1.8984375
- w_branch: bfloat16 [1024, 512], P(None, 'tp'), may hold values from -0.1875 to 0.1875
- w_gate: bfloat16 [1024, 512], P(None, 'tp'), may hold values from -0.1875 to 0.1875
- conv_taps: bfloat16 [4, 512], P(None, 'tp'), may hold values from -3 to 3
- w_recur: bfloat16 [8, 64, 64], P('tp'), may hold values from -0.75 to 0.75
- w_inject: bfloat16 [8, 64, 64], P('tp'), may hold values from -0.75 to 0.75
- lru_lambda: float32 [512], P('tp'), may hold values from 2 to 7
- w_out: bfloat16 [512, 1024], P('tp'), may hold values from -0.25 to 0.25
- expert_gate: bfloat16 [128, 1024, 2560], P('ep', None, 'tp'), may hold values from -0.1875 to 0.1875
- expert_up: bfloat16 [128, 1024, 2560], P('ep', None, 'tp'), may hold values from -0.1875 to 0.1875
- expert_down: bfloat16 [128, 2560, 1024], P('ep', 'tp'), may hold values from -0.125 to 0.125
- route_ids: int32 [8192, 2], P('ep'), may hold values from 0 to 127, all different within a row; in each aligned block of 64 rows (0 to 63, 64 to 127, ...) at most 2 rows name the same one
- route_weight: float32 [8192, 2], P('ep'), may hold values from 0.2 to 1
Outputs:
- mixed: bfloat16 [8192, 1024], P('ep', 'tp')
- state_out: float32 [8192, 512], P('ep', 'tp')
Inputs may be any that keep to these rules, and one draw needn't show every extreme that they name: `route_ids`: each row names 2 different experts. Among the 64 rows of one device no expert is named more than 2 times, and in every draw some expert is named exactly 2 times by them.
All inputs are finite; a program needn't handle non-finite values.
Results may differ from a plain program's by a relative error of at most 0.015.
Values may be sent and summed in bfloat16 or wider, within the bound.
A program may use at most 64 MiB of HBM per device.

v0:
```python
import jax
import jax.numpy as jnp
from jax import lax
from jax.sharding import PartitionSpec as P

EPS = 1e-06
LRU_SCALE = 8.0


def joined_along(pieces, dim):
    pieces = jnp.moveaxis(pieces, 0, dim)
    lengths = pieces.shape
    return pieces.reshape(*lengths[:dim], lengths[dim] * lengths[dim + 1], *lengths[dim + 2 :])


def sent_to_all(x, axis):
    count = lax.axis_size(axis)
    return lax.all_to_all(jnp.broadcast_to(x[None], (count, *x.shape)), axis, 0, 0, tiled=True)


def gathered_copies(x, axis, dim):
    return joined_along(sent_to_all(x, axis), dim)


def in_blocks(x, dim, count):
    lengths = x.shape
    pieces = x.reshape(*lengths[:dim], count, lengths[dim] // count, *lengths[dim + 1 :])
    return jnp.moveaxis(pieces, dim, 0)


def sent_and_summed(x, axis, dim):
    pieces = in_blocks(x, dim, lax.axis_size(axis))
    arrived = lax.all_to_all(pieces, axis, split_axis=0, concat_axis=0, tiled=True)
    return arrived.astype(jnp.float32).sum(axis=0)


def rms_rows(rows, gain):
    values = rows.astype(jnp.float32)
    scaled = values * lax.rsqrt(jnp.mean(values * values, axis=-1, keepdims=True) + EPS)
    return (scaled * gain.astype(jnp.float32)).astype(jnp.bfloat16)


def body(
    tokens,
    conv_state,
    lru_state,
    mix_gain,
    ffn_gain,
    w_branch,
    w_gate,
    conv_taps,
    w_recur,
    w_inject,
    lru_lambda,
    w_out,
    expert_gate,
    expert_up,
    expert_down,
    route_ids,
    route_weight,
):
    seqs = tokens.shape[0]
    whole = gathered_copies(tokens, "tp", 1)
    normed = rms_rows(whole, mix_gain)
    branch = jnp.dot(normed, w_branch, preferred_element_type=jnp.float32).astype(jnp.bfloat16)
    gate_in = jnp.dot(normed, w_gate, preferred_element_type=jnp.float32).astype(jnp.bfloat16)
    window = jnp.concatenate([conv_state, branch[:, None, :]], axis=1).astype(jnp.float32)
    conv_out = jnp.sum(window * conv_taps.astype(jnp.float32)[None], axis=1)
    heads_here = w_recur.shape[0]
    head_width = w_recur.shape[1]
    conv_heads = conv_out.astype(jnp.bfloat16).reshape(seqs, heads_here, head_width)
    recur = jax.nn.sigmoid(
        jnp.einsum("nhi,hij->nhj", conv_heads, w_recur, preferred_element_type=jnp.float32).reshape(
            seqs, -1
        )
    )
    inject = jax.nn.sigmoid(
        jnp.einsum(
            "nhi,hij->nhj", conv_heads, w_inject, preferred_element_type=jnp.float32
        ).reshape(seqs, -1)
    )
    log_decay = -LRU_SCALE * recur * jax.nn.softplus(-lru_lambda)
    state_out = (
        jnp.exp(log_decay) * lru_state + jnp.sqrt(-jnp.expm1(2.0 * log_decay)) * inject * conv_out
    )
    lru_out = (state_out * jax.nn.gelu(gate_in.astype(jnp.float32))).astype(jnp.bfloat16)
    partial_value = jnp.dot(lru_out, w_out, preferred_element_type=jnp.float32)
    partial_value = lax.optimization_barrier(partial_value.astype(jnp.bfloat16)).astype(jnp.float32)
    mix_out = sent_and_summed(partial_value.astype(jnp.bfloat16), "tp", 1).astype(jnp.bfloat16)
    resid = (tokens.astype(jnp.float32) + mix_out.astype(jnp.float32)).astype(jnp.bfloat16)
    top = route_ids.shape[1]
    local = expert_gate.shape[0]
    experts = lax.axis_size("ep") * local
    capacity = max(2, 2 * seqs * top // experts)
    flat = route_ids.reshape(-1)
    onehot = (flat[:, None] == jnp.arange(experts, dtype=jnp.int32)[None, :]).astype(jnp.int32)
    before = jnp.cumsum(onehot, axis=0) - onehot
    slot = jnp.sum(before * onehot, axis=1)
    slot_id = slot * experts + flat
    places = jnp.arange(capacity * experts, dtype=jnp.int32)
    hits = slot_id[None, :] == places[:, None]
    dispatch = jnp.sum(
        hits.reshape(capacity * experts, seqs, top).astype(jnp.float32), axis=2
    ).astype(jnp.bfloat16)
    spread = jnp.transpose(hits).reshape(seqs, top, capacity * experts)
    combine = jnp.sum(jnp.where(spread, route_weight[:, :, None], 0.0), axis=1)
    full = gathered_copies(resid, "tp", 1)
    normed2 = rms_rows(full, ffn_gain)
    buffer = jnp.dot(dispatch, normed2, preferred_element_type=jnp.float32).astype(jnp.bfloat16)
    buffer = buffer.reshape(capacity, experts, -1)
    block = lax.all_to_all(buffer, "ep", split_axis=1, concat_axis=1, tiled=True)
    count = block.shape[0]
    width = block.shape[2]
    grid = block.reshape(count, -1, local, width)
    rows = grid[:, :, 0].reshape(-1, width)
    first = jnp.dot(rows, expert_gate[0], preferred_element_type=jnp.float32)
    second = jnp.dot(rows, expert_up[0], preferred_element_type=jnp.float32)
    hidden = (jax.nn.silu(first) * second).astype(jnp.bfloat16)
    term = jnp.dot(hidden, expert_down[0], preferred_element_type=jnp.float32)
    term = lax.optimization_barrier(term.astype(jnp.bfloat16)).astype(jnp.float32)
    summed = sent_and_summed(term.astype(jnp.bfloat16), "tp", 1).astype(jnp.bfloat16)
    results = summed.reshape(count, -1, 1, summed.shape[1])
    answered = results.reshape(count, -1, results.shape[3])
    returned = lax.all_to_all(answered, "ep", split_axis=1, concat_axis=1, tiled=True)
    back = returned.reshape(capacity * experts, -1).astype(jnp.float32)
    moe = jnp.dot(combine, back)
    mixed = (resid.astype(jnp.float32) + moe).astype(jnp.bfloat16)
    return (mixed, state_out)


def solution(mesh):
    placed = (
        P("ep", "tp"),
        P("ep", None, "tp"),
        P("ep", "tp"),
        P(),
        P(),
        P(None, "tp"),
        P(None, "tp"),
        P(None, "tp"),
        P("tp", None, None),
        P("tp", None, None),
        P("tp"),
        P("tp", None),
        P("ep", None, "tp"),
        P("ep", None, "tp"),
        P("ep", "tp", None),
        P("ep", None),
        P("ep", None),
    )
    return jax.shard_map(
        body, mesh=mesh, in_specs=placed, out_specs=(P("ep", "tp"), P("ep", "tp")), check_vma=False
    )
```

profile of v0, /device:TPU:1, one launch (start us, length us, event | category | flops | bytes accessed | tf_op | source)
XLA Modules:
  0.0 109.8 jit_solution(5886516992850330418)
XLA Ops:
  0.6 0.0 copy-start
  0.7 1.5 %broadcast_in_dim.14 = bf16[4,64,256]{2,1,0:T(8,128)(2,1)} broadcast(bf16[64,256]{1,0:T(8,128)(2,1)} %param.17), dimensions={1,2} | broadcast | bytes 163840 | tf_op jit(solution)/shard_map/broadcast_in_dim | solution.py:18
  2.2 4.8 %all-to-all-start = ((bf16[4,64,256]{2,1,0:T(8,128)(2,1)}), bf16[4,64,256]{2,1,0:T(8,128)(2,1)S(1)}, u32[]{:S(2)}, u32[]{:S(2)}) async-start(bf16[4,64,256]{2,1,0:T(8,128)(2,1)} %broadcast_in_dim.14), calls=%async_computation | async-start | bytes 262144 | tf_op jit(solution)/shard_map/all_to_all | solution.py:18
  7.0 0.7 convert_element_type.113
  7.7 0.7 convert_element_type.117
  8.4 0.7 fusion.55
  9.1 0.8 copy.80
  9.8 0.1 eq.37
  10.0 0.0 copy-start.13
  10.0 0.1 fusion.38
  10.1 0.2 reduce_window_sum.11
  10.2 0.2 select_reduce_fusion.1
  10.4 1.4 %all-to-all-done = bf16[4,64,256]{2,1,0:T(8,128)(2,1)S(1)} async-done(((bf16[4,64,256]{2,1,0:T(8,128)(2,1)}), bf16[4,64,256]{2,1,0:T(8,128)(2,1)S(1)}, u32[]{:S(2)}, u32[]{:S(2)}) %all-to-all-start) | async-done | bytes 131104 | tf_op jit(solution)/shard_map/all_to_all | solution.py:18
  11.9 0.1 fusion.34
  12.1 0.2 fusion.27
  12.4 0.1 convert_element_type.119
  12.5 0.1 fusion.24
  12.7 0.1 copy.76
  12.7 0.1 div.24
  12.8 0.1 fusion.20
  13.0 0.1 copy.78
  13.0 0.1 div.26
  13.2 0.0 copy-start.6
  13.2 0.4 convolution_convert_fusion.1
  13.6 0.6 copy.99
  14.3 3.3 %all-to-all-start.1 = ((bf16[4,64,256]{2,1,0:T(8,128)(2,1)}), bf16[4,64,256]{2,1,0:T(8,128)(2,1)S(1)}, u32[]{:S(2)}, u32[]{:S(2)}) async-start(bf16[4,64,256]{2,1,0:T(8,128)(2,1)} %bitcast.58), calls=%async_computation.1 | async-start | bytes 262144 | tf_op jit(solution)/shard_map/all_to_all | solution.py:33
  17.6 0.1 mul.153
  17.7 0.1 copy.81
  17.8 0.0 copy-done.10
  17.8 4.5 %all-to-all-done.1 = bf16[4,64,256]{2,1,0:T(8,128)(2,1)S(1)} async-done(((bf16[4,64,256]{2,1,0:T(8,128)(2,1)}), bf16[4,64,256]{2,1,0:T(8,128)(2,1)S(1)}, u32[]{:S(2)}, u32[]{:S(2)}) %all-to-all-start.1) | async-done | bytes 131104 | tf_op jit(solution)/shard_map/all_to_all | solution.py:33
  22.4 0.6 broadcast_in_dim.22
  23.1 3.3 %all-to-all-start.2 = ((bf16[4,64,256]{2,1,0:T(8,128)(2,1)}), bf16[4,64,256]{2,1,0:T(8,128)(2,1)S(1)}, u32[]{:S(2)}, u32[]{:S(2)}) async-start(bf16[4,64,256]{2,1,0:T(8,128)(2,1)} %broadcast_in_dim.22), calls=%async_computation.2 | async-start | bytes 262144 | tf_op jit(solution)/shard_map/all_to_all | solution.py:18
  26.4 0.1 convert_reduce_fusion
  26.5 4.7 %all-to-all-done.2 = bf16[4,64,256]{2,1,0:T(8,128)(2,1)S(1)} async-done(((bf16[4,64,256]{2,1,0:T(8,128)(2,1)}), bf16[4,64,256]{2,1,0:T(8,128)(2,1)S(1)}, u32[]{:S(2)}, u32[]{:S(2)}) %all-to-all-start.2) | async-done | bytes 131104 | tf_op jit(solution)/shard_map/all_to_all | solution.py:18
  31.3 0.1 fusion.35
  31.4 0.4 convolution_convert_fusion
  31.8 0.5 copy.83
  32.3 41.8 %all_to_all.30 = bf16[2,128,1024]{2,0,1:T(2,128)(2,1)S(1)} all-to-all(bf16[2,128,1024]{2,0,1:T(2,128)(2,1)S(1)} %copy.83), channel_id=1, replica_groups=mesh['ep'=128,'tp'=4] {'ep'}, dimensions={1} | all-to-all | bytes 1048576 | tf_op jit(solution)/shard_map/all_to_all | solution.py:111
  74.1 0.1 copy.84
  74.3 0.6 fusion.4
  74.9 2.4 %fusion.6 = bf16[256,1024]{1,0:T(8,128)(2,1)S(1)} fusion(bf16[1,640,1024]{2,1,0:T(8,128)(2,1)S(1)} %copy-done, bf16[256,1024]{1,0:T(8,128)(2,1)S(1)} %bitcast.62, bf16[1,1024,640]{2,1,0:T(8,128)(2,1)} %param.30, f32[256,640]{1,0:T(8,128)S(1)} %fusion.4), kind=kOutput, calls=%fused_computation.6 | convolution fusion | flops 672333824 | bytes 4325376 | tf_op jit(solution)/shard_map/dot_general | solution.py:119
  77.3 12.2 %all_to_all.31 = bf16[4,256,256]{2,1,0:T(8,128)(2,1)S(1)} all-to-all(bf16[4,256,256]{2,1,0:T(8,128)(2,1)S(1)} %bitcast.64), channel_id=1, replica_groups=mesh['ep'=128,'tp'=4] {'tp'}, dimensions={0} | all-to-all | bytes 1048576 | tf_op jit(solution)/shard_map/all_to_all | solution.py:33
  89.5 0.1 reduce_sum.85
  89.6 0.8 copy.86
  90.4 5.8 %all-to-all-start.5 = ((bf16[2,128,256]{2,0,1:T(2,128)(2,1)}), bf16[2,128,256]{2,0,1:T(2,128)(2,1)S(1)}, u32[]{:S(2)}, u32[]{:S(2)}) async-start(bf16[2,128,256]{2,0,1:T(2,128)(2,1)} %copy.86), calls=%async_computation.5 | async-start | bytes 262144 | tf_op jit(solution)/shard_map/all_to_all | solution.py:124
  96.2 0.1 select_reduce_fusion
  96.3 12.7 %all-to-all-done.5 = bf16[2,128,256]{2,0,1:T(2,128)(2,1)S(1)} async-done(((bf16[2,128,256]{2,0,1:T(2,128)(2,1)}), bf16[2,128,256]{2,0,1:T(2,128)(2,1)S(1)}, u32[]{:S(2)}, u32[]{:S(2)}) %all-to-all-start.5) | async-done | bytes 131104 | tf_op jit(solution)/shard_map/all_to_all | solution.py:124
  109.0 0.8 fusion.25
  (40 shorter events, 0.3 us)
Async XLA Ops:
  0.6 74.2 %copy-start = (bf16[1,640,1024]{2,1,0:T(8,128)(2,1)S(1)}, bf16[1,640,1024]{2,1,0:T(8,128)(2,1)}, u32[]{:S(2)}) copy-start(bf16[1,640,1024]{2,1,0:T(8,128)(2,1)} %param.31) | copy-start | bytes 3932164
  0.6 11.4 %copy-start.4 = (bf16[1024,128]{1,0:T(8,128)(2,1)S(1)}, bf16[1024,128]{1,0:T(8,128)(2,1)}, u32[]{:S(2)}) copy-start(bf16[1024,128]{1,0:T(8,128)(2,1)} %param.22) | copy-start | bytes 786436
  0.7 11.7 %copy-start.7 = (bf16[64,3,128]{2,0,1:T(8,128)(2,1)S(1)}, bf16[64,3,128]{2,0,1:T(8,128)(2,1)}, u32[]{:S(2)}) copy-start(bf16[64,3,128]{2,0,1:T(8,128)(2,1)} %param.18) | copy-start | bytes 147460
  0.7 11.8 %copy-start.12 = (bf16[2,64,64]{2,1,0:T(8,128)(2,1)S(1)}, bf16[2,64,64]{2,1,0:T(8,128)(2,1)}, u32[]{:S(2)}) copy-start(bf16[2,64,64]{2,1,0:T(8,128)(2,1)} %param.25) | copy-start | bytes 49156
  2.2 9.7 %all-to-all-start = ((bf16[4,64,256]{2,1,0:T(8,128)(2,1)}), bf16[4,64,256]{2,1,0:T(8,128)(2,1)S(1)}, u32[]{:S(2)}, u32[]{:S(2)}) async-start(bf16[4,64,256]{2,1,0:T(8,128)(2,1)} %broadcast_in_dim.14), calls=%async_computation | async-start | bytes 262144 | tf_op jit(solution)/shard_map/all_to_all | solution.py:18
  10.0 2.8 %copy-start.13 = (bf16[2,64,64]{2,1,0:T(8,128)(2,1)S(1)}, bf16[2,64,64]{2,1,0:T(8,128)(2,1)}, u32[]{:S(2)}) copy-start(bf16[2,64,64]{2,1,0:T(8,128)(2,1)} %param.26) | copy-start | bytes 49156
  11.9 1.3 %copy-start.8 = (f32[64,128]{1,0:T(8,128)S(1)}, f32[64,128]{1,0:T(8,128)}, u32[]{:S(2)}) copy-start(f32[64,128]{1,0:T(8,128)} %param.19) | copy-start | bytes 98308
  11.9 1.3 %copy-start.2 = (bf16[128,1024]{1,0:T(8,128)(2,1)S(1)}, bf16[128,1024]{1,0:T(8,128)(2,1)}, u32[]{:S(2)}) copy-start(bf16[128,1024]{1,0:T(8,128)(2,1)} %param.28) | copy-start | bytes 786436
  11.9 1.3 %copy-start.3 = (bf16[1024,128]{1,0:T(8,128)(2,1)S(1)}, bf16[1024,128]{1,0:T(8,128)(2,1)}, u32[]{:S(2)}) copy-start(bf16[1024,128]{1,0:T(8,128)(2,1)} %param.23) | copy-start | bytes 786436
  12.6 5.2 %copy-start.9 = (s32[64,2]{0,1:T(2,128)S(1)}, s32[64,2]{0,1:T(2,128)}, u32[]{:S(2)}) copy-start(s32[64,2]{0,1:T(2,128)} %param.32) | copy-start | bytes 1540
  12.6 5.2 %copy-start.10 = (bf16[1024]{0:T(1024)(128)(2,1)S(1)}, bf16[1024]{0:T(1024)(128)(2,1)}, u32[]{:S(2)}) copy-start(bf16[1024]{0:T(1024)(128)(2,1)} %param.21) | copy-start | bytes 6148
  12.6 9.8 %copy-start.5 = (bf16[64,256]{1,0:T(8,128)(2,1)S(1)}, bf16[64,256]{1,0:T(8,128)(2,1)}, u32[]{:S(2)}) copy-start(bf16[64,256]{1,0:T(8,128)(2,1)} %param.17) | copy-start | bytes 98308
  13.2 18.0 %copy-start.6 = (f32[64,128]{1,0:T(8,128)}, f32[64,128]{1,0:T(8,128)S(1)}, u32[]{:S(2)}) copy-start(f32[64,128]{1,0:T(8,128)S(1)} %multiply_add_fusion) | copy-start | bytes 98308
  14.3 8.1 %all-to-all-start.1 = ((bf16[4,64,256]{2,1,0:T(8,128)(2,1)}), bf16[4,64,256]{2,1,0:T(8,128)(2,1)S(1)}, u32[]{:S(2)}, u32[]{:S(2)}) async-start(bf16[4,64,256]{2,1,0:T(8,128)(2,1)} %bitcast.58), calls=%async_computation.1 | async-start | bytes 262144 | tf_op jit(solution)/shard_map/all_to_all | solution.py:33
  23.1 8.1 %all-to-all-start.2 = ((bf16[4,64,256]{2,1,0:T(8,128)(2,1)}), bf16[4,64,256]{2,1,0:T(8,128)(2,1)S(1)}, u32[]{:S(2)}, u32[]{:S(2)}) async-start(bf16[4,64,256]{2,1,0:T(8,128)(2,1)} %broadcast_in_dim.22), calls=%async_computation.2 | async-start | bytes 262144 | tf_op jit(solution)/shard_map/all_to_all | solution.py:18
  32.3 41.9 %copy-start.1 = (bf16[1,1024,640]{2,1,0:T(8,128)(2,1)S(1)}, bf16[1,1024,640]{2,1,0:T(8,128)(2,1)}, u32[]{:S(2)}) copy-start(bf16[1,1024,640]{2,1,0:T(8,128)(2,1)} %param.29) | copy-start | bytes 3932164
  77.3 18.9 %copy-start.11 = (f32[64,2]{0,1:T(2,128)S(1)}, f32[64,2]{0,1:T(2,128)}, u32[]{:S(2)}) copy-start(f32[64,2]{0,1:T(2,128)} %param.33) | copy-start | bytes 1540
  90.4 18.6 %all-to-all-start.5 = ((bf16[2,128,256]{2,0,1:T(2,128)(2,1)}), bf16[2,128,256]{2,0,1:T(2,128)(2,1)S(1)}, u32[]{:S(2)}, u32[]{:S(2)}) async-start(bf16[2,128,256]{2,0,1:T(2,128)(2,1)} %copy.86), calls=%async_computation.5 | async-start | bytes 262144 | tf_op jit(solution)/shard_map/all_to_all | solution.py:124
where the time goes:
time: 110 us
  blocking collectives  54 us (49%)
  waiting for transfers between devices  23.4 us (21%)
  starting transfers between devices  17.3 us (16%)
  local copies, waits for them, and re-layouts  5.92 us (5%)
  matrix products  5.02 us (5%)
  other arithmetic  3.14 us (3%)
    all_to_all x1, blocking collectives, body(): lax.all_to_all(buffer, 'ep', split_axis=1, concat_axis=1, tiled=True)  41.8 us
    all_to_all x1, waiting for transfers between devices, body(): lax.all_to_all(answered, 'ep', split_axis=1, concat_axis=1, tiled=True)  12.7 us
    all_to_all x1, blocking collectives, sent_and_summed(): lax.all_to_all(pieces, axis, split_axis=0, concat_axis=0, tiled=True)  12.2 us
    all_to_all x2, starting transfers between devices, sent_to_all(): lax.all_to_all(jnp.broadcast_to(x[None], (count, *x.shape)), axis, 0, 0,...  8.15 us
    all_to_all x2, waiting for transfers between devices, sent_to_all(): lax.all_to_all(jnp.broadcast_to(x[None], (count, *x.shape)), axis, 0, 0,...  6.13 us
    all_to_all x1, starting transfers between devices, body(): lax.all_to_all(answered, 'ep', split_axis=1, concat_axis=1, tiled=True)  5.77 us
    all_to_all x1, waiting for transfers between devices, sent_and_summed(): lax.all_to_all(pieces, axis, split_axis=0, concat_axis=0, tiled=True)  4.54 us
    all_to_all x1, starting transfers between devices, sent_and_summed(): lax.all_to_all(pieces, axis, split_axis=0, concat_axis=0, tiled=True)  3.32 us
  transfers between devices with their start and end apart: 4, of which 4 were waited for; matrix products, arithmetic and copies ran while one was open for 3% of the time, Pallas kernels for 0%

commit v1 on v0

--- a/solution.py
+++ b/solution.py
@@ -121,7 +121,10 @@
     summed = sent_and_summed(term.astype(jnp.bfloat16), "tp", 1).astype(jnp.bfloat16)
     results = summed.reshape(count, -1, 1, summed.shape[1])
     answered = results.reshape(count, -1, results.shape[3])
-    returned = lax.all_to_all(answered, "ep", split_axis=1, concat_axis=1, tiled=True)
+    returned = jnp.concatenate(
+        lax.all_to_all(jnp.stack(jnp.split(answered, lax.axis_size("ep"), axis=1)), "ep", 0, 0),
+        axis=1,
+    )
     back = returned.reshape(capacity * experts, -1).astype(jnp.float32)
     moe = jnp.dot(combine, back)
     mixed = (resid.astype(jnp.float32) + moe).astype(jnp.bfloat16)

time: 110 us -> 184 us (1.67)
  local copies, waits for them, and re-layouts: 5.92 us -> 79.4 us
    unnamed x29 -> x156, local copies, waits for them, and re-layouts: 0.87 us -> 73.8 us
  transfers between devices with their start and end apart: 4 -> 4, of which waited for: 4 -> 4; matrix products, arithmetic and copies ran while one was open for 3% -> 2% of each run, Pallas kernels for 0% -> 0%
where the time goes in v1:
time: 184 us; the launch traced here: 183 us
  local copies, waits for them, and re-layouts  79.4 us (43%)
  blocking collectives  54 us (29%)
  waiting for transfers between devices  23.4 us (13%)
  starting transfers between devices  17.2 us (9%)
  matrix products  5.03 us (3%)
  other arithmetic  3.14 us (2%)
    unnamed x156, local copies, waits for them, and re-layouts  73.8 us
    all_to_all x1, blocking collectives, body(): lax.all_to_all(buffer, 'ep', split_axis=1, concat_axis=1, tiled=True)  41.8 us
    all_to_all x1, waiting for transfers between devices, body(): lax.all_to_all(jnp.stack(jnp.split(answered, lax.axis_size('ep'), axis=1)...  12.7 us
    all_to_all x1, blocking collectives, sent_and_summed(): lax.all_to_all(pieces, axis, split_axis=0, concat_axis=0, tiled=True)  12.2 us
    all_to_all x2, starting transfers between devices, sent_to_all(): lax.all_to_all(jnp.broadcast_to(x[None], (count, *x.shape)), axis, 0, 0,...  8.15 us
    all_to_all x2, waiting for transfers between devices, sent_to_all(): lax.all_to_all(jnp.broadcast_to(x[None], (count, *x.shape)), axis, 0, 0,...  6.13 us
    all_to_all x1, starting transfers between devices, body(): lax.all_to_all(jnp.stack(jnp.split(answered, lax.axis_size('ep'), axis=1)...  5.75 us
    all_to_all x1, waiting for transfers between devices, sent_and_summed(): lax.all_to_all(pieces, axis, split_axis=0, concat_axis=0, tiled=True)  4.54 us
  transfers between devices with their start and end apart: 4, of which 4 were waited for; matrix products, arithmetic and copies ran while one was open for 2% of the time, Pallas kernels for 0%

profile of v1, /device:TPU:1, one launch (start us, length us, event | category | flops | bytes accessed | tf_op | source)
XLA Modules:
  0.0 183.4 jit_solution(1384869663402579028)
XLA Ops:
  0.7 1.5 broadcast_in_dim.14
  2.2 4.8 %all-to-all-start = ((bf16[4,64,256]{2,1,0:T(8,128)(2,1)}), bf16[4,64,256]{2,1,0:T(8,128)(2,1)S(1)}, u32[]{:S(2)}, u32[]{:S(2)}) async-start(bf16[4,64,256]{2,1,0:T(8,128)(2,1)} %broadcast_in_dim.14), calls=%async_computation | async-start | bytes 262144 | tf_op jit(solution)/shard_map/all_to_all | solution.py:18
  7.0 0.7 convert_element_type.113
  7.7 0.7 convert_element_type.117
  8.4 0.7 fusion.55
  9.1 0.8 copy.3682
  10.4 1.4 all-to-all-done
  13.7 0.7 copy.3681
  14.4 3.3 %all-to-all-start.1 = ((bf16[4,64,256]{2,1,0:T(8,128)(2,1)}), bf16[4,64,256]{2,1,0:T(8,128)(2,1)S(1)}, u32[]{:S(2)}, u32[]{:S(2)}) async-start(bf16[4,64,256]{2,1,0:T(8,128)(2,1)} %copy.3681), calls=%async_computation.1 | async-start | bytes 262144 | tf_op jit(solution)/shard_map/all_to_all | solution.py:33
  17.9 4.5 %all-to-all-done.1 = bf16[4,64,256]{2,1,0:T(8,128)(2,1)S(1)} async-done(((bf16[4,64,256]{2,1,0:T(8,128)(2,1)}), bf16[4,64,256]{2,1,0:T(8,128)(2,1)S(1)}, u32[]{:S(2)}, u32[]{:S(2)}) %all-to-all-start.1) | async-done | bytes 131104 | tf_op jit(solution)/shard_map/all_to_all | solution.py:33
  22.5 0.7 broadcast_in_dim.22
  23.2 3.3 %all-to-all-start.2 = ((bf16[4,64,256]{2,1,0:T(8,128)(2,1)}), bf16[4,64,256]{2,1,0:T(8,128)(2,1)S(1)}, u32[]{:S(2)}, u32[]{:S(2)}) async-start(bf16[4,64,256]{2,1,0:T(8,128)(2,1)} %broadcast_in_dim.22), calls=%async_computation.2 | async-start | bytes 262144 | tf_op jit(solution)/shard_map/all_to_all | solution.py:18
  26.6 4.7 %all-to-all-done.2 = bf16[4,64,256]{2,1,0:T(8,128)(2,1)S(1)} async-done(((bf16[4,64,256]{2,1,0:T(8,128)(2,1)}), bf16[4,64,256]{2,1,0:T(8,128)(2,1)S(1)}, u32[]{:S(2)}, u32[]{:S(2)}) %all-to-all-start.2) | async-done | bytes 131104 | tf_op jit(solution)/shard_map/all_to_all | solution.py:18
  32.4 41.8 %all_to_all.30 = bf16[2,128,1024]{2,0,1:T(2,128)(2,1)S(1)} all-to-all(bf16[2,128,1024]{2,0,1:T(2,128)(2,1)S(1)} %copy.3685), channel_id=1, replica_groups=mesh['ep'=128,'tp'=4] {'ep'}, dimensions={1} | all-to-all | bytes 1048576 | tf_op jit(solution)/shard_map/all_to_all | solution.py:111
  75.0 2.4 %fusion.6 = bf16[256,1024]{1,0:T(8,128)(2,1)S(1)} fusion(bf16[1,640,1024]{2,1,0:T(8,128)(2,1)S(1)} %copy-done, bf16[256,1024]{1,0:T(8,128)(2,1)S(1)} %bitcast.307, bf16[1,1024,640]{2,1,0:T(8,128)(2,1)} %param.30, f32[256,640]{1,0:T(8,128)S(1)} %fusion.4), kind=kOutput, calls=%fused_computation.6 | convolution fusion | flops 672333824 | bytes 4325376 | tf_op jit(solution)/shard_map/dot_general | solution.py:119
  77.8 12.2 %all_to_all.31 = bf16[4,256,256]{2,1,0:T(8,128)(2,1)S(1)} all-to-all(bf16[4,256,256]{2,1,0:T(8,128)(2,1)S(1)} %copy.3687), channel_id=1, replica_groups=mesh['ep'=128,'tp'=4] {'tp'}, dimensions={0} | all-to-all | bytes 1048576 | tf_op jit(solution)/shard_map/all_to_all | solution.py:33
  91.6 0.6 constant_dynamic-update-slice_fusion.125
  92.2 0.6 constant_dynamic-update-slice_fusion.124
  93.9 0.6 constant_dynamic-update-slice_fusion.121
  100.8 0.6 constant_dynamic-update-slice_fusion.109
  103.6 0.6 constant_dynamic-update-slice_fusion.104
  104.2 0.6 constant_dynamic-update-slice_fusion.103
  106.5 0.6 constant_dynamic-update-slice_fusion.99
  107.1 0.6 constant_dynamic-update-slice_fusion.98
  110.0 0.6 constant_dynamic-update-slice_fusion.93
  110.6 0.6 constant_dynamic-update-slice_fusion.92
  112.9 0.6 constant_dynamic-update-slice_fusion.88
  118.6 0.6 constant_dynamic-update-slice_fusion.78
  124.4 0.6 constant_dynamic-update-slice_fusion.68
  126.1 0.6 constant_dynamic-update-slice_fusion.65
  126.7 0.6 constant_dynamic-update-slice_fusion.64
  127.3 0.6 constant_dynamic-update-slice_fusion.63
  127.9 0.6 constant_dynamic-update-slice_fusion.62
  129.6 0.6 constant_dynamic-update-slice_fusion.59
  130.2 0.6 constant_dynamic-update-slice_fusion.58
  133.7 0.6 constant_dynamic-update-slice_fusion.52
  139.3 0.6 constant_dynamic-update-slice_fusion.42
  140.5 0.6 constant_dynamic-update-slice_fusion.40
  144.5 0.6 constant_dynamic-update-slice_fusion.33
  146.3 0.6 constant_dynamic-update-slice_fusion.30
  148.0 0.6 constant_dynamic-update-slice_fusion.27
  152.0 0.6 constant_dynamic-update-slice_fusion.20
  158.9 0.6 constant_dynamic-update-slice_fusion.8
  161.7 0.6 constant_dynamic-update-slice_fusion.3
  162.3 0.6 constant_dynamic-update-slice_fusion.2
  164.1 5.8 %all-to-all-start.5 = ((bf16[128,2,1,256]{3,1,2,0:T(2,128)(2,1)}), bf16[128,2,1,256]{3,1,2,0:T(2,128)(2,1)S(1)}, u32[]{:S(2)}, u32[]{:S(2)}) async-start(bf16[128,2,1,256]{3,1,2,0:T(2,128)(2,1)} %constant_dynamic-update-slice_fusion), calls=%async_computation.5 | async-start | bytes 262144 | tf_op jit(solution)/shard_map/all_to_all | solution.py:125
  169.9 12.7 %all-to-all-done.5 = bf16[128,2,1,256]{3,1,2,0:T(2,128)(2,1)S(1)} async-done(((bf16[128,2,1,256]{3,1,2,0:T(2,128)(2,1)}), bf16[128,2,1,256]{3,1,2,0:T(2,128)(2,1)S(1)}, u32[]{:S(2)}, u32[]{:S(2)}) %all-to-all-start.5) | async-done | bytes 131104 | tf_op jit(solution)/shard_map/all_to_all | solution.py:125
  182.7 0.8 fusion.25
  (176 shorter events, 61.6 us)
Async XLA Ops:
  0.6 74.3 %copy-start = (bf16[1,640,1024]{2,1,0:T(8,128)(2,1)S(1)}, bf16[1,640,1024]{2,1,0:T(8,128)(2,1)}, u32[]{:S(2)}) copy-start(bf16[1,640,1024]{2,1,0:T(8,128)(2,1)} %param.31) | copy-start | bytes 3932164
  0.6 11.4 %copy-start.4 = (bf16[1024,128]{1,0:T(8,128)(2,1)S(1)}, bf16[1024,128]{1,0:T(8,128)(2,1)}, u32[]{:S(2)}) copy-start(bf16[1024,128]{1,0:T(8,128)(2,1)} %param.22) | copy-start | bytes 786436
  0.7 11.7 %copy-start.7 = (bf16[64,3,128]{2,0,1:T(8,128)(2,1)S(1)}, bf16[64,3,128]{2,0,1:T(8,128)(2,1)}, u32[]{:S(2)}) copy-start(bf16[64,3,128]{2,0,1:T(8,128)(2,1)} %param.18) | copy-start | bytes 147460
  0.7 11.8 %copy-start.12 = (bf16[2,64,64]{2,1,0:T(8,128)(2,1)S(1)}, bf16[2,64,64]{2,1,0:T(8,128)(2,1)}, u32[]{:S(2)}) copy-start(bf16[2,64,64]{2,1,0:T(8,128)(2,1)} %param.25) | copy-start | bytes 49156
  2.2 9.7 %all-to-all-start = ((bf16[4,64,256]{2,1,0:T(8,128)(2,1)}), bf16[4,64,256]{2,1,0:T(8,128)(2,1)S(1)}, u32[]{:S(2)}, u32[]{:S(2)}) async-start(bf16[4,64,256]{2,1,0:T(8,128)(2,1)} %broadcast_in_dim.14), calls=%async_computation | async-start | bytes 262144 | tf_op jit(solution)/shard_map/all_to_all | solution.py:18
  10.0 2.8 %copy-start.13 = (bf16[2,64,64]{2,1,0:T(8,128)(2,1)S(1)}, bf16[2,64,64]{2,1,0:T(8,128)(2,1)}, u32[]{:S(2)}) copy-start(bf16[2,64,64]{2,1,0:T(8,128)(2,1)} %param.26) | copy-start | bytes 49156
  11.9 1.2 copy-start.8
  11.9 1.3 copy-start.2
  11.9 1.3 copy-start.3
  12.7 5.2 %copy-start.9 = (s32[64,2]{0,1:T(2,128)S(1)}, s32[64,2]{0,1:T(2,128)}, u32[]{:S(2)}) copy-start(s32[64,2]{0,1:T(2,128)} %param.32) | copy-start | bytes 1540
  12.7 5.2 %copy-start.10 = (bf16[1024]{0:T(1024)(128)(2,1)S(1)}, bf16[1024]{0:T(1024)(128)(2,1)}, u32[]{:S(2)}) copy-start(bf16[1024]{0:T(1024)(128)(2,1)} %param.21) | copy-start | bytes 6148
  12.8 9.7 %copy-start.5 = (bf16[64,256]{1,0:T(8,128)(2,1)S(1)}, bf16[64,256]{1,0:T(8,128)(2,1)}, u32[]{:S(2)}) copy-start(bf16[64,256]{1,0:T(8,128)(2,1)} %param.17) | copy-start | bytes 98308
  13.2 18.1 %copy-start.6 = (f32[64,128]{1,0:T(8,128)}, f32[64,128]{1,0:T(8,128)S(1)}, u32[]{:S(2)}) copy-start(f32[64,128]{1,0:T(8,128)S(1)} %multiply_add_fusion) | copy-start | bytes 98308
  14.4 8.1 %all-to-all-start.1 = ((bf16[4,64,256]{2,1,0:T(8,128)(2,1)}), bf16[4,64,256]{2,1,0:T(8,128)(2,1)S(1)}, u32[]{:S(2)}, u32[]{:S(2)}) async-start(bf16[4,64,256]{2,1,0:T(8,128)(2,1)} %copy.3681), calls=%async_computation.1 | async-start | bytes 262144 | tf_op jit(solution)/shard_map/all_to_all | solution.py:33
  23.2 8.1 %all-to-all-start.2 = ((bf16[4,64,256]{2,1,0:T(8,128)(2,1)}), bf16[4,64,256]{2,1,0:T(8,128)(2,1)S(1)}, u32[]{:S(2)}, u32[]{:S(2)}) async-start(bf16[4,64,256]{2,1,0:T(8,128)(2,1)} %broadcast_in_dim.22), calls=%async_computation.2 | async-start | bytes 262144 | tf_op jit(solution)/shard_map/all_to_all | solution.py:18
  32.4 41.9 %copy-start.1 = (bf16[1,1024,640]{2,1,0:T(8,128)(2,1)S(1)}, bf16[1,1024,640]{2,1,0:T(8,128)(2,1)}, u32[]{:S(2)}) copy-start(bf16[1,1024,640]{2,1,0:T(8,128)(2,1)} %param.29) | copy-start | bytes 3932164
  77.8 92.0 %copy-start.11 = (f32[64,2]{0,1:T(2,128)S(1)}, f32[64,2]{0,1:T(2,128)}, u32[]{:S(2)}) copy-start(f32[64,2]{0,1:T(2,128)} %param.33) | copy-start | bytes 1540
  164.1 18.6 %all-to-all-start.5 = ((bf16[128,2,1,256]{3,1,2,0:T(2,128)(2,1)}), bf16[128,2,1,256]{3,1,2,0:T(2,128)(2,1)S(1)}, u32[]{:S(2)}, u32[]{:S(2)}) async-start(bf16[128,2,1,256]{3,1,2,0:T(2,128)(2,1)} %constant_dynamic-update-slice_fusion), calls=%async_computation.5 | async-start | bytes 262144 | tf_op jit(solution)/shard_map/all_to_all | solution.py:125
